TPU v7x, 256 devices: a 4x2x16 block of a 4x16x16 slice. The times are simulated.
256 devices in a mesh: grp: 2 (over y), fs: 16 (over z), tp: 8 (over x, core).
Axes of the slice: x: 4, y: 2, z: 16, core: 2. Of those that a mesh axis runs over, the one named last changes fastest.
The devices are a block of a 4x16x16 slice.
Arguments:
- layer_input: bfloat16 [12288, 2048], P(('grp', 'fs'), 'tp'), parts along dimension 0, may hold values from -6 to 6
- first_gain: bfloat16 [1, 2048], P(None, 'tp'), may hold values from 0.099609375 to 1.8984375
- ffn_gate_w: bfloat16 [2048, 6144], P('fs', 'tp'), may hold values from -0.125 to 0.125
- ffn_up_w: bfloat16 [2048, 6144], P('fs', 'tp'), may hold values from -0.125 to 0.125
- ffn_down_w: bfloat16 [6144, 2048], P('tp', 'fs'), may hold values from -0.078125 to 0.078125
- mixer_gain: bfloat16 [1, 2048], P(None, 'tp'), may hold values from 0.099609375 to 1.8984375
- pool_in_w: bfloat16 [2048, 1024], P('fs', 'tp'), may hold values from -0.125 to 0.125
- mixer_gate_w: bfloat16 [2048, 2048], P('fs', 'tp'), may hold values from -0.125 to 0.125
- group_mix_w: bfloat16 [8, 128, 128], P('tp'), may hold values from -0.5 to 0.5
- pool_scale: float32 [1, 1024], P(None, 'tp'), may hold values from 0.1 to 1.9
- mixer_out_w: bfloat16 [1024, 2048], P('tp', 'fs'), may hold values from -0.1875 to 0.1875
- second_gain: bfloat16 [1, 2048], P(None, 'tp'), may hold values from 0.099609375 to 1.8984375
Outputs:
- layer_output: bfloat16 [12288, 2048], P(('grp', 'fs'), 'tp'), parts along dimension 0
There are 2 independent parts, one for each index of `grp`. A program takes and returns all parts, laid end to end along the dimension named above; an argument that names none is the same for every part. Nothing has to cross between parts.
All inputs are finite; a program needn't handle non-finite values.
Results may differ from a plain program's by a relative error of at most 0.015.
Values may be sent and summed in bfloat16 or wider, within the bound.
A program may use at most 64 MiB of HBM per device.

v0:
```python
import jax
import jax.numpy as jnp
from jax import lax
from jax.sharding import Mesh
from jax.sharding import PartitionSpec as P

TP = ("tp_0", "tp_1")


def from_everyone(value, axis):
    length = lax.axis_size(axis)
    return lax.all_to_all(
        jnp.broadcast_to(value[None], (length, *value.shape)), axis, 0, 0, tiled=True
    )


def joined_along(tiles, dim):
    shape = list(tiles.shape[1:])
    shape[dim] *= tiles.shape[0]
    return jnp.moveaxis(tiles, 0, dim).reshape(shape)


def whole_of(value, axes, dim):
    far, near = axes
    initial = from_everyone(value, far)
    tiles = jnp.swapaxes(from_everyone(initial, near), 0, 1)
    return joined_along(tiles.reshape(-1, *value.shape), dim)


def in_one_piece(arrays, axis, dim, along):
    widths = [a.shape[along] for a in arrays]
    both = jnp.concatenate(arrays, axis=along)
    filled = whole_of(both, axis, dim)
    return tuple(jnp.split(filled, [sum(widths[:k]) for k in range(1, len(widths))], axis=along))


def in_blocks(value, dim, length):
    before, after = (value.shape[:dim], value.shape[dim + 1 :])
    return jnp.moveaxis(value.reshape(*before, length, -1, *after), dim, 0)


def summed_on_arrival(value, axis, dim):
    tiles = in_blocks(value, dim, lax.axis_size(axis))
    arrived = lax.all_to_all(tiles, axis, split_axis=0, concat_axis=0, tiled=True)
    return arrived.astype(jnp.float32).sum(axis=0)


def sent_together(arrays, axis, dim, along):
    ends, at = ([], 0)
    for a in arrays[:-1]:
        at += a.shape[along]
        ends.append(at)
    both = jnp.concatenate(arrays, axis=along)
    return tuple(jnp.split(lax.all_gather(both, axis, axis=dim, tiled=True), ends, axis=along))


def gather_directly(value, axis, dim):
    return joined_along(from_everyone(value, axis), dim)


def norm_rows(values, gain):
    gathered, gain_whole = in_one_piece((values, gain), ("tp_0", "tp_1"), 1, 0)
    widened = gathered.astype(jnp.float32)
    scaled = (widened * gain_whole.astype(jnp.float32)).astype(jnp.bfloat16)
    factor = lax.rsqrt(jnp.mean(widened * widened, axis=1, keepdims=True) + 1e-06)
    return (scaled, factor)


def column_sums(partial_value):
    return summed_on_arrival(partial_value.astype(jnp.bfloat16), TP, 1)


def add_pair(scaled, pieces):
    first_sum = jnp.dot(scaled, pieces[0], preferred_element_type=jnp.float32)
    second_sum = jnp.dot(scaled, pieces[1], preferred_element_type=jnp.float32)
    return (first_sum, second_sum)


def per_device(
    layer_input,
    first_gain,
    ffn_gate_w,
    ffn_up_w,
    ffn_down_w,
    mixer_gain,
    pool_in_w,
    mixer_gate_w,
    group_mix_w,
    pool_scale,
    mixer_out_w,
    second_gain,
):
    row_count = layer_input.shape[0]
    gate_whole, up_whole = sent_together((ffn_gate_w, ffn_up_w), "fs", 0, 1)
    down_whole = lax.all_gather(ffn_down_w, "fs", axis=1, tiled=True)

    def feed_forward(values, gain):
        scaled, factor = norm_rows(values, gain)
        gate_pre = factor * jnp.dot(scaled, gate_whole, preferred_element_type=jnp.float32)
        up_pre = factor * jnp.dot(scaled, up_whole, preferred_element_type=jnp.float32)
        hidden = (jax.nn.silu(gate_pre) * up_pre).astype(jnp.bfloat16)
        return jnp.dot(hidden, down_whole, preferred_element_type=jnp.float32)

    first = (
        layer_input.astype(jnp.float32) + 0.5 * column_sums(feed_forward(layer_input, first_gain))
    ).astype(jnp.bfloat16)
    scaled, factor = norm_rows(first, mixer_gain)
    pool_sum, gate_sum = add_pair(scaled, sent_together((pool_in_w, mixer_gate_w), "fs", 0, 1))
    pool_pre = (factor * pool_sum).astype(jnp.bfloat16)
    gate_logit = factor * gate_sum
    group_count = group_mix_w.shape[0]
    group_width = group_mix_w.shape[1]
    first_group = lax.axis_index(TP) * group_count
    values = pool_pre.astype(jnp.float32).reshape(row_count, group_count, group_width)
    running = jnp.cumsum(values, axis=0)
    positions = jnp.arange(row_count, dtype=jnp.int32)
    windows = 2 ** (1 + (first_group + jnp.arange(group_count, dtype=jnp.int32)) % 4)
    chosen = jnp.zeros_like(values)
    for span in (2, 4, 8, 16):
        lagged = jnp.pad(running, ((span, 0), (0, 0), (0, 0)))[:row_count]
        counts = jnp.minimum(positions + 1, span).astype(jnp.float32)[:, None, None]
        means = (running - lagged) / counts
        chosen = jnp.where((windows == span)[None, :, None], means, chosen)
    trail = (chosen - values).astype(jnp.bfloat16)
    mixed = jnp.einsum("tgc,gcd->tgd", trail, group_mix_w, preferred_element_type=jnp.float32)
    pooled = (mixed.reshape(row_count, group_count * group_width) * pool_scale).astype(jnp.bfloat16)
    lifted = column_sums(
        jnp.dot(pooled, gather_directly(mixer_out_w, "fs", 1), preferred_element_type=jnp.float32)
    )
    second = (first.astype(jnp.float32) + jax.nn.sigmoid(gate_logit) * lifted).astype(jnp.bfloat16)
    result = second.astype(jnp.float32) + 0.5 * column_sums(feed_forward(second, second_gain))
    return result.astype(jnp.bfloat16)


def solution(mesh):
    finer = Mesh(
        mesh.devices.reshape(mesh.shape["grp"], mesh.shape["fs"], 4, 2),
        ("grp", "fs", "tp_0", "tp_1"),
    )
    return jax.shard_map(
        per_device,
        mesh=finer,
        in_specs=(
            P(("grp", "fs"), TP),
            P(None, TP),
            P("fs", TP),
            P("fs", TP),
            P(TP, "fs"),
            P(None, TP),
            P("fs", TP),
            P("fs", TP),
            P(TP, None, None),
            P(None, TP),
            P(TP, "fs"),
            P(None, TP),
        ),
        out_specs=P(("grp", "fs"), TP),
        check_vma=False,
    )
```

profile of v0, /device:TPU:33, one launch (start us, length us, event | category | flops | bytes accessed | tf_op | source)
XLA Modules:
  0.0 387.3 jit_solution(81376959434211735)
XLA Ops:
  6.6 1.8 pad_maximum_fusion
  8.5 0.7 all-gather.6.cloned.1.call-update
  9.2 1.0 pad_maximum_fusion.1
  10.3 13.3 %all_to_all.50 = bf16[4,385,256]{2,1,0:T(8,128)(2,1)S(1)} all-to-all(bf16[4,385,256]{2,1,0:T(8,128)(2,1)S(1)} %broadcast_in_dim.91), channel_id=1, replica_groups=mesh['grp'=2,'fs'=16,'tp_0'=4,'tp_1'=2] {'tp_0'}, dimensions={0} | all-to-all | bytes 1576960 | tf_op jit(solution)/shard_map/all_to_all | solution.py:12
  23.9 0.4 broadcast_in_dim.92
  24.3 23.7 %all_to_all.51 = bf16[2,4,385,256]{3,1,2,0:T(4,128)(2,1)S(1)} all-to-all(bf16[2,4,385,256]{3,1,2,0:T(4,128)(2,1)S(1)} %broadcast_in_dim.92), channel_id=1, replica_groups=mesh['grp'=2,'fs'=16,'tp_0'=4,'tp_1'=2] {'tp_1'}, dimensions={0} | all-to-all | bytes 3153920 | tf_op jit(solution)/shard_map/all_to_all | solution.py:12
  48.2 1.9 slice_convert_fusion.2
  50.2 3.6 copy.35
  54.1 2.3 fusion.2
  56.4 48.7 %all-gather.4.cloned.1.call-done = bf16[2048,1536]{1,0:T(8,128)(2,1)} async-done(((bf16[128,1536]{1,0:T(8,128)(2,1)}), bf16[2048,1536]{1,0:T(8,128)(2,1)}) %all-gather.4.cloned.1.call-update) | async-done | bytes 6291472 | tf_op jit(solution)/shard_map/all_gather | solution.py:54
  105.1 4.3 %fusion.11 = f32[384,768]{1,0:T(8,128)} fusion(bf16[384,2048]{0,1:T(8,128)(2,1)S(1)} %fusion.2, bf16[2048,1536]{1,0:T(8,128)(2,1)} %all-gather.4.cloned.1.call-done, f32[384]{0:T(512)S(1)} %add_rsqrt_fusion.2), kind=kOutput, calls=%fused_computation.29 | convolution fusion | flops 1208254464 | bytes 5899776 | tf_op jit(solution)/shard_map/dot_general | solution.py:99
  109.4 71.1 %all-gather.6.cloned.1.call-done = bf16[768,2048]{1,0:T(8,128)(2,1)} async-done(((bf16[768,128]{1,0:T(8,128)(2,1)}), bf16[768,2048]{1,0:T(8,128)(2,1)}) %all-gather.6.cloned.1.call-update) | async-done | bytes 3145744 | tf_op jit(solution)/shard_map/all_gather | solution.py:95
  180.5 6.4 %convolution_convert_fusion.1 = bf16[384,2048]{1,0:T(8,128)(2,1)S(1)} fusion(bf16[768,2048]{1,0:T(8,128)(2,1)} %all-gather.6.cloned.1.call-done, bf16[384,2048]{0,1:T(8,128)(2,1)S(1)} %fusion.2, bf16[2048,1536]{1,0:T(8,128)(2,1)} %all-gather.4.cloned.1.call-done, f32[384,768]{1,0:T(8,128)} %fusion.11, f32[384]{0:T(512)S(1)} %add_rsqrt_fusion.2), kind=kOutput, calls=%fused_computation.13 | convolution fusion | flops 2418769920 | bytes 10618368 | tf_op jit(solution)/shard_map/dot_general | solution.py:102
  186.9 1.3 copy.58
  188.1 15.3 %all-to-all-start.2 = ((bf16[8,384,256]{2,1,0:T(8,128)(2,1)}), bf16[8,384,256]{2,1,0:T(8,128)(2,1)S(1)}, u32[]{:S(2)}, u32[]{:S(2)}) async-start(bf16[8,384,256]{2,1,0:T(8,128)(2,1)} %bitcast.111), calls=%async_computation.2 | async-start | bytes 3145728 | tf_op jit(solution)/shard_map/all_to_all | solution.py:44
  203.5 0.7 pad_maximum_fusion.4
  204.2 19.8 %all-to-all-done.2 = bf16[8,384,256]{2,1,0:T(8,128)(2,1)S(1)} async-done(((bf16[8,384,256]{2,1,0:T(8,128)(2,1)}), bf16[8,384,256]{2,1,0:T(8,128)(2,1)S(1)}, u32[]{:S(2)}, u32[]{:S(2)}) %all-to-all-start.2) | async-done | bytes 1572896 | tf_op jit(solution)/shard_map/all_to_all | solution.py:44
  224.4 0.9 broadcast_in_dim.93
  225.3 3.6 all-to-all-start.3
  229.1 11.3 %all-to-all-done.3 = bf16[4,385,256]{2,1,0:T(8,128)(2,1)S(1)} async-done(((bf16[4,385,256]{2,1,0:T(8,128)(2,1)}), bf16[4,385,256]{2,1,0:T(8,128)(2,1)S(1)}, u32[]{:S(2)}, u32[]{:S(2)}) %all-to-all-start.3) | async-done | bytes 788512 | tf_op jit(solution)/shard_map/all_to_all | solution.py:12
  240.7 0.4 broadcast_in_dim.94
  241.1 6.5 %all_to_all.52 = bf16[2,4,385,256]{3,1,2,0:T(4,128)(2,1)S(1)} all-to-all(bf16[2,4,385,256]{3,1,2,0:T(4,128)(2,1)S(1)} %broadcast_in_dim.94), channel_id=1, replica_groups=mesh['grp'=2,'fs'=16,'tp_0'=4,'tp_1'=2] {'tp_1'}, dimensions={0} | all-to-all | bytes 3153920 | tf_op jit(solution)/shard_map/all_to_all | solution.py:12
  247.6 0.9 broadcast_in_dim.104
  248.5 7.0 %all-to-all-start.5 = ((bf16[16,128,128]{1,2,0:T(8,128)(2,1)}), bf16[16,128,128]{1,2,0:T(8,128)(2,1)}, u32[]{:S(2)}, u32[]{:S(2)}) async-start(bf16[16,128,128]{1,2,0:T(8,128)(2,1)} %broadcast_in_dim.104), calls=%async_computation.5 | async-start | bytes 1048576 | tf_op jit(solution)/shard_map/all_to_all | solution.py:12
  255.7 1.9 slice_convert_fusion.1
  257.6 3.5 copy.39
  261.5 2.2 fusion.1
  263.8 3.6 all-gather.8.cloned.1.call-done
  267.4 1.6 fusion.47
  269.1 0.7 copy-done.6
  270.0 0.7 fusion.73
  270.7 10.8 %all-to-all-done.5 = bf16[16,128,128]{1,2,0:T(8,128)(2,1)} async-done(((bf16[16,128,128]{1,2,0:T(8,128)(2,1)}), bf16[16,128,128]{1,2,0:T(8,128)(2,1)}, u32[]{:S(2)}, u32[]{:S(2)}) %all-to-all-start.5) | async-done | bytes 524320 | tf_op jit(solution)/shard_map/all_to_all | solution.py:12
  281.5 2.4 convolution_convert_fusion.2
  284.0 31.3 %all_to_all.53 = bf16[8,384,256]{2,1,0:T(8,128)(2,1)S(1)} all-to-all(bf16[8,384,256]{2,1,0:T(8,128)(2,1)S(1)} %bitcast.125), channel_id=1, replica_groups=mesh['grp'=2,'fs'=16,'tp_0'=4,'tp_1'=2] {'tp_0','tp_1'}, dimensions={0} | all-to-all | bytes 3145728 | tf_op jit(solution)/shard_map/all_to_all | solution.py:44
  315.5 1.2 copy-done.12
  316.7 0.7 fusion.41
  317.4 0.6 copy-done.4
  318.1 13.9 %all_to_all.54 = bf16[4,385,256]{2,1,0:T(8,128)(2,1)S(1)} all-to-all(bf16[4,385,256]{2,1,0:T(8,128)(2,1)S(1)} %broadcast_in_dim.105), channel_id=1, replica_groups=mesh['grp'=2,'fs'=16,'tp_0'=4,'tp_1'=2] {'tp_0'}, dimensions={0} | all-to-all | bytes 1576960 | tf_op jit(solution)/shard_map/all_to_all | solution.py:12
  332.3 0.4 broadcast_in_dim.106
  332.7 6.5 %all_to_all.55 = bf16[2,4,385,256]{3,1,2,0:T(4,128)(2,1)S(1)} all-to-all(bf16[2,4,385,256]{3,1,2,0:T(4,128)(2,1)S(1)} %broadcast_in_dim.106), channel_id=1, replica_groups=mesh['grp'=2,'fs'=16,'tp_0'=4,'tp_1'=2] {'tp_1'}, dimensions={0} | all-to-all | bytes 3153920 | tf_op jit(solution)/shard_map/all_to_all | solution.py:12
  339.5 1.9 slice_convert_fusion
  341.8 2.4 copy.46
  344.6 1.2 copy-done.2
  345.7 3.3 fusion.14
  349.1 6.5 %convolution_convert_fusion = bf16[384,2048]{1,0:T(8,128)(2,1)S(1)} fusion(bf16[768,2048]{1,0:T(8,128)(2,1)} %all-gather.6.cloned.1.call-done, bf16[384,2048]{0,1:T(8,128)(2,1)} %copy-done.2, bf16[2048,1536]{1,0:T(8,128)(2,1)} %all-gather.4.cloned.1.call-done, f32[384,768]{1,0:T(8,128)S(1)} %fusion.14, f32[384]{0:T(512)S(1)} %add_rsqrt_fusion), kind=kOutput, calls=%fused_computation.12 | convolution fusion | flops 2418769920 | bytes 10618368 | tf_op jit(solution)/shard_map/dot_general | solution.py:102
  355.7 23.4 %all_to_all.56 = bf16[8,384,256]{2,1,0:T(8,128)(2,1)S(1)} all-to-all(bf16[8,384,256]{2,1,0:T(8,128)(2,1)S(1)} %bitcast.126), channel_id=1, replica_groups=mesh['grp'=2,'fs'=16,'tp_0'=4,'tp_1'=2] {'tp_0','tp_1'}, dimensions={0} | all-to-all | bytes 3145728 | tf_op jit(solution)/shard_map/all_to_all | solution.py:44
  379.3 0.7 copy-done.5
  380.0 0.7 add_convert_fusion
  (63 shorter events, 4.8 us)
Async XLA Ops:
  6.5 275.0 %copy-start = (bf16[1,128,128]{2,1,0:T(8,128)(2,1)S(1)}, bf16[1,128,128]{2,1,0:T(8,128)(2,1)}, u32[]{:S(2)}) copy-start(bf16[1,128,128]{2,1,0:T(8,128)(2,1)} %param.20) | copy-start | bytes 98308
  6.6 98.6 %all-gather.4.cloned.1.call-start = ((), (), s32[]{:S(2)}) async-start(), calls=%async_computation.10 | async-start | bytes 6684672 | tf_op jit(solution)/shard_map/all_gather | solution.py:54
  8.4 172.1 %all-gather.6.cloned.1.call-start = ((), (), s32[]{:S(2)}) async-start(), calls=%async_computation.11 | async-start | bytes 3342336 | tf_op jit(solution)/shard_map/all_gather | solution.py:95
  188.1 15.4 %copy-start.7 = (bf16[128,256]{1,0:T(8,128)(2,1)S(1)}, bf16[128,256]{1,0:T(8,128)(2,1)}, u32[]{:S(2)}) copy-start(bf16[128,256]{1,0:T(8,128)(2,1)} %param.19) | copy-start | bytes 196612
  188.1 15.4 %copy-start.9 = (bf16[128,128]{1,0:T(8,128)(2,1)S(1)}, bf16[128,128]{1,0:T(8,128)(2,1)}, u32[]{:S(2)}) copy-start(bf16[128,128]{1,0:T(8,128)(2,1)} %param.18) | copy-start | bytes 98308
  188.1 35.9 %all-to-all-start.2 = ((bf16[8,384,256]{2,1,0:T(8,128)(2,1)}), bf16[8,384,256]{2,1,0:T(8,128)(2,1)S(1)}, u32[]{:S(2)}, u32[]{:S(2)}) async-start(bf16[8,384,256]{2,1,0:T(8,128)(2,1)} %bitcast.111), calls=%async_computation.2 | async-start | bytes 3145728 | tf_op jit(solution)/shard_map/all_to_all | solution.py:44
  203.4 20.8 %copy-start.3 = (bf16[384,256]{1,0:T(8,128)(2,1)S(1)}, bf16[384,256]{1,0:T(8,128)(2,1)}, u32[]{:S(2)}) copy-start(bf16[384,256]{1,0:T(8,128)(2,1)} %param.12) | copy-start | bytes 589828
  203.4 20.9 %copy-start.10 = (bf16[1,256]{1,0:T(2,128)(2,1)S(1)}, bf16[1,256]{1,0:T(2,128)(2,1)}, u32[]{:S(2)}) copy-start(bf16[1,256]{1,0:T(2,128)(2,1)} %param.17) | copy-start | bytes 1540
  203.4 64.0 %all-gather.8.cloned.1.call-start = ((), (), s32[]{:S(2)}) async-start(), calls=%async_computation.12 | async-start | bytes 1671168 | tf_op jit(solution)/shard_map/all_gather | solution.py:54
  224.3 4.6 %copy-start.8 = (bf16[128,128]{1,0:T(8,128)(2,1)S(1)}, bf16[128,128]{1,0:T(8,128)(2,1)}, u32[]{:S(2)}) copy-start(bf16[128,128]{1,0:T(8,128)(2,1)} %param.22) | copy-start | bytes 98308
  225.3 15.1 %all-to-all-start.3 = ((bf16[4,385,256]{2,1,0:T(8,128)(2,1)}), bf16[4,385,256]{2,1,0:T(8,128)(2,1)S(1)}, u32[]{:S(2)}, u32[]{:S(2)}) async-start(bf16[4,385,256]{2,1,0:T(8,128)(2,1)} %broadcast_in_dim.93), calls=%async_computation.3 | async-start | bytes 1605632 | tf_op jit(solution)/shard_map/all_to_all | solution.py:12
  248.5 33.0 %all-to-all-start.5 = ((bf16[16,128,128]{1,2,0:T(8,128)(2,1)}), bf16[16,128,128]{1,2,0:T(8,128)(2,1)}, u32[]{:S(2)}, u32[]{:S(2)}) async-start(bf16[16,128,128]{1,2,0:T(8,128)(2,1)} %broadcast_in_dim.104), calls=%async_computation.5 | async-start | bytes 1048576 | tf_op jit(solution)/shard_map/all_to_all | solution.py:12
  269.1 0.7 copy-start.6
  269.1 12.4 %copy-start.13 = (f32[1,128]{1,0:T(1,128)S(1)}, f32[1,128]{1,0:T(1,128)}, u32[]{:S(2)}) copy-start(f32[1,128]{1,0:T(1,128)} %param.21) | copy-start | bytes 1540
  315.3 1.4 copy-start.12
  316.7 0.7 copy-start.11
  317.4 0.7 copy-start.4
  344.6 1.2 copy-start.2
  355.7 25.1 %copy-start.1 = (bf16[1,128,128]{2,1,0:T(8,128)(2,1)S(1)}, bf16[1,128,128]{2,1,0:T(8,128)(2,1)}, u32[]{:S(2)}) copy-start(bf16[1,128,128]{2,1,0:T(8,128)(2,1)} %param.20) | copy-start | bytes 98308
  379.1 0.9 copy-start.5
Sparse Core Ops, SparseCore 0:
  9.1 95.9 all-gather.3
  106.8 73.5 all-gather.5
  206.1 61.3 all-gather.7
where the time goes:
time: 388 us; the launch traced here: 387 us
  waiting for transfers between devices  166 us (43%)
  blocking collectives  119 us (31%)
  starting transfers between devices  26 us (7%)
  matrix products  25.2 us (6%)
  local copies, waits for them, and re-layouts  20.2 us (5%)
  other arithmetic  17.6 us (5%)
  between operations  13.6 us (4%)
    all_gather x1, waiting for transfers between devices, per_device(): down_whole = lax.all_gather(ffn_down_w, 'fs', axis=1, tiled=True)  71.1 us
    all_to_all x5, blocking collectives, from_everyone(): lax.all_to_all(jnp.broadcast_to(value[None], (length, *value.shape)), axi...  64 us
    all_to_all x2, blocking collectives, summed_on_arrival(): lax.all_to_all(tiles, axis, split_axis=0, concat_axis=0, tiled=True)  54.7 us
    all_gather x2, waiting for transfers between devices, sent_together(): lax.all_gather(both, axis, axis=dim, tiled=True)  52.3 us
    all_to_all x2, waiting for transfers between devices, from_everyone(): lax.all_to_all(jnp.broadcast_to(value[None], (length, *value.shape)), axi...  22.1 us
    all_to_all x1, waiting for transfers between devices, summed_on_arrival(): lax.all_to_all(tiles, axis, split_axis=0, concat_axis=0, tiled=True)  19.8 us
    all_to_all x1, starting transfers between devices, summed_on_arrival(): lax.all_to_all(tiles, axis, split_axis=0, concat_axis=0, tiled=True)  15.3 us
    dot_general x2, matrix products, feed_forward(): return jnp.dot(hidden, down_whole, preferred_element_type=jnp.float32)  12.9 us
  transfers between devices with their start and end apart: 6, of which 6 were waited for; matrix products, arithmetic and copies ran while one was open for 7% of the time, Pallas kernels for 0%

commit v1 on v0

--- a/solution.py
+++ b/solution.py
@@ -5,6 +5,12 @@
 from jax.sharding import PartitionSpec as P
 
 TP = ("tp_0", "tp_1")
+
+
+def in_order(pieces, dim):
+    shape = list(pieces.shape[1:])
+    shape[dim] *= pieces.shape[0]
+    return jnp.moveaxis(pieces, 0, dim).reshape(shape)
 
 
 def from_everyone(value, axis):
@@ -92,7 +98,19 @@
 ):
     row_count = layer_input.shape[0]
     gate_whole, up_whole = sent_together((ffn_gate_w, ffn_up_w), "fs", 0, 1)
-    down_whole = lax.all_gather(ffn_down_w, "fs", axis=1, tiled=True)
+    size = lax.axis_size("fs")
+    pairs = [(i, (i + 1) % size) for i in range(size)]
+    back = [(b, a_2) for a_2, b in pairs]
+    lower, upper = ([], [])
+    for turn in range(size - 1):
+        if turn % 2 == 0:
+            lower.append(lax.ppermute(lower[-1] if lower else ffn_down_w, "fs", pairs))
+        else:
+            upper.append(lax.ppermute(upper[-1] if upper else ffn_down_w, "fs", back))
+    blocks = jnp.stack([*lower[::-1], ffn_down_w, *upper])
+    shift = lax.axis_index("fs") - len(lower)
+    blocks = blocks[(jnp.arange(size) - shift) % size]
+    down_whole = in_order(blocks, 1)
 
     def feed_forward(values, gain):
         scaled, factor = norm_rows(values, gain)

time: 388 us -> 348 us (0.90)
  waiting for transfers between devices: 166 us -> 97.6 us
  starting transfers between devices: 26 us -> 58.7 us
  blocking collectives: 119 us -> 91.1 us
  local copies, waits for them, and re-layouts: 20.2 us -> 39.1 us
    all_gather x1 -> x0, waiting for transfers between devices: 71.1 us -> none  [per_device(): down_whole = lax.all_gather(ffn_down_w, 'fs', axis=1, tiled=True)]
    ppermute x0 -> x15, waiting for transfers between devices: none -> 52.1 us  [the longest x8 50 us: per_device(): lower.append(lax.ppermute(lower[-1] if lower else ffn_down_w, 'fs', pairs))]
    all_gather x2, waiting for transfers between devices: 52.3 us -> 3.18 us  [sent_together(): lax.all_gather(both, axis, axis=dim, tiled=True)]
    ppermute x0 -> x15, starting transfers between devices: none -> 38.1 us  [the longest x7 33.8 us: per_device(): upper.append(lax.ppermute(upper[-1] if upper else ffn_down_w, 'fs', back))]
    all_to_all x5 -> x4, blocking collectives: 64 us -> 36.9 us  [from_everyone(): lax.all_to_all(jnp.broadcast_to(value[None], (length, *value.shape)), axi...]
    unnamed x29 -> x48, local copies, waits for them, and re-layouts: 4.51 us -> 13 us
    all_to_all x1, starting transfers between devices: 15.3 us -> 7.86 us  [summed_on_arrival(): lax.all_to_all(tiles, axis, split_axis=0, concat_axis=0, tiled=True)]
    all_to_all x2 -> x3, starting transfers between devices: 10.5 us -> 12.7 us  [from_everyone(): lax.all_to_all(jnp.broadcast_to(value[None], (length, *value.shape)), axi...]
  transfers between devices with their start and end apart: 6 -> 21, of which waited for: 6 -> 12; matrix products, arithmetic and copies ran while one was open for 7% -> 13% of each run, Pallas kernels for 0% -> 0%
where the time goes in v1:
time: 348 us; the launch traced here: 347 us
  waiting for transfers between devices  97.6 us (28%)
  blocking collectives  91.1 us (26%)
  starting transfers between devices  58.7 us (17%)
  local copies, waits for them, and re-layouts  39.1 us (11%)
  matrix products  28.2 us (8%)
  other arithmetic  18.8 us (5%)
  between operations  13.9 us (4%)
    all_to_all x2, blocking collectives, summed_on_arrival(): lax.all_to_all(tiles, axis, split_axis=0, concat_axis=0, tiled=True)  54.2 us
    ppermute x8, waiting for transfers between devices, per_device(): lower.append(lax.ppermute(lower[-1] if lower else ffn_down_w, 'fs', pairs))  50 us
    all_to_all x4, blocking collectives, from_everyone(): lax.all_to_all(jnp.broadcast_to(value[None], (length, *value.shape)), axi...  36.9 us
    ppermute x7, starting transfers between devices, per_device(): upper.append(lax.ppermute(upper[-1] if upper else ffn_down_w, 'fs', back))  33.8 us
    all_to_all x3, waiting for transfers between devices, from_everyone(): lax.all_to_all(jnp.broadcast_to(value[None], (length, *value.shape)), axi...  22.4 us
    all_to_all x1, waiting for transfers between devices, summed_on_arrival(): lax.all_to_all(tiles, axis, split_axis=0, concat_axis=0, tiled=True)  19.8 us
    dot_general x2, matrix products, feed_forward(): return jnp.dot(hidden, down_whole, preferred_element_type=jnp.float32)  14 us
    unnamed x48, local copies, waits for them, and re-layouts  13 us
  transfers between devices with their start and end apart: 21, of which 12 were waited for; matrix products, arithmetic and copies ran while one was open for 13% of the time, Pallas kernels for 0%

profile of v1, /device:TPU:33, one launch (start us, length us, event | category | flops | bytes accessed | tf_op | source)
XLA Modules:
  0.0 347.4 jit_solution(13590517608033294383)
XLA Ops:
  6.6 1.8 pad_maximum_fusion
  8.4 3.4 collective-permute-start
  11.9 19.7 %collective-permute-start.8 = (bf16[768,128]{1,0:T(8,128)(2,1)}, bf16[768,128]{1,0:T(8,128)(2,1)S(1)}, u32[]{:S(2)}, u32[]{:S(2)}) collective-permute-start(bf16[768,128]{1,0:T(8,128)(2,1)} %param.16), channel_id=1, source_target_pairs={{8,0},{16,8},{24,16},{32,24},{40,32},{48,40},{56,48},{64,56},{72,6... | collective-permute-start | bytes 589832 | tf_op jit(solution)/shard_map/ppermute | solution.py:109
  33.5 4.3 %all-to-all-start = ((bf16[4,385,256]{2,1,0:T(8,128)(2,1)}), bf16[4,385,256]{2,1,0:T(8,128)(2,1)S(1)}, u32[]{:S(2)}, u32[]{:S(2)}) async-start(bf16[4,385,256]{2,1,0:T(8,128)(2,1)} %broadcast_in_dim.92), calls=%async_computation | async-start | bytes 1605632 | tf_op jit(solution)/shard_map/all_to_all | solution.py:18
  37.9 2.7 collective-permute-start.9
  40.5 6.2 %collective-permute-done.1 = bf16[768,128]{1,0:T(8,128)(2,1)S(1)} collective-permute-done((bf16[768,128]{1,0:T(8,128)(2,1)S(1)}, bf16[768,128]{1,0:T(8,128)(2,1)S(1)}, u32[]{:S(2)}, u32[]{:S(2)}) %collective-permute-start.1) | collective-permute-done | bytes 196640 | tf_op jit(solution)/shard_map/ppermute | solution.py:107
  48.5 1.2 collective-permute-start.10
  49.6 8.2 %collective-permute-done.2 = bf16[768,128]{1,0:T(8,128)(2,1)S(1)} collective-permute-done((bf16[768,128]{1,0:T(8,128)(2,1)S(1)}, bf16[768,128]{1,0:T(8,128)(2,1)S(1)}, u32[]{:S(2)}, u32[]{:S(2)}) %collective-permute-start.2) | collective-permute-done | bytes 196640 | tf_op jit(solution)/shard_map/ppermute | solution.py:107
  57.8 1.1 collective-permute-done.10
  59.0 1.5 collective-permute-start.11
  61.2 9.9 %all_to_all.50 = bf16[2,4,385,256]{3,1,2,0:T(4,128)(2,1)S(1)} all-to-all(bf16[2,4,385,256]{3,1,2,0:T(4,128)(2,1)S(1)} %broadcast_in_dim.93), channel_id=1, replica_groups=mesh['grp'=2,'fs'=16,'tp_0'=4,'tp_1'=2] {'tp_1'}, dimensions={0} | all-to-all | bytes 3153920 | tf_op jit(solution)/shard_map/all_to_all | solution.py:18
  71.4 1.9 slice_convert_fusion.2
  73.3 3.7 %copy.43 = f32[384,8,256]{0,2,1:T(8,128)} copy(f32[384,8,256]{2,0,1:T(8,128)} %slice_convert_fusion.2) | data formatting | bytes 6291456 | tf_op jit(solution)/shard_map/convert_element_type | solution.py:69
  77.0 12.3 %collective-permute-done.4 = bf16[768,128]{1,0:T(8,128)(2,1)S(1)} collective-permute-done((bf16[768,128]{1,0:T(8,128)(2,1)S(1)}, bf16[768,128]{1,0:T(8,128)(2,1)S(1)}, u32[]{:S(2)}, u32[]{:S(2)}) %collective-permute-start.4) | collective-permute-done | bytes 196640 | tf_op jit(solution)/shard_map/ppermute | solution.py:107
  89.4 3.4 fusion.2
  92.7 2.7 collective-permute-start.12
  95.4 6.1 %collective-permute-done.5 = bf16[768,128]{1,0:T(8,128)(2,1)S(1)} collective-permute-done((bf16[768,128]{1,0:T(8,128)(2,1)S(1)}, bf16[768,128]{1,0:T(8,128)(2,1)S(1)}, u32[]{:S(2)}, u32[]{:S(2)}) %collective-permute-start.5) | collective-permute-done | bytes 196640 | tf_op jit(solution)/shard_map/ppermute | solution.py:107
  101.9 3.1 collective-permute-start.13
  105.0 8.4 %collective-permute-done.6 = bf16[768,128]{1,0:T(8,128)(2,1)S(1)} collective-permute-done((bf16[768,128]{1,0:T(8,128)(2,1)S(1)}, bf16[768,128]{1,0:T(8,128)(2,1)S(1)}, u32[]{:S(2)}, u32[]{:S(2)}) %collective-permute-start.6) | collective-permute-done | bytes 196640 | tf_op jit(solution)/shard_map/ppermute | solution.py:107
  113.4 2.9 collective-permute-start.14
  116.3 8.8 %collective-permute-done.7 = bf16[768,128]{1,0:T(8,128)(2,1)S(1)} collective-permute-done((bf16[768,128]{1,0:T(8,128)(2,1)S(1)}, bf16[768,128]{1,0:T(8,128)(2,1)S(1)}, u32[]{:S(2)}, u32[]{:S(2)}) %collective-permute-start.7) | collective-permute-done | bytes 196640 | tf_op jit(solution)/shard_map/ppermute | solution.py:107
  136.3 3.0 gather_fusion
  139.3 2.9 copy.44
  142.2 5.0 %fusion.11 = f32[384,768]{1,0:T(8,128)} fusion(bf16[384,2048]{0,1:T(8,128)(2,1)} %fusion.2, bf16[2048,1536]{1,0:T(8,128)(2,1)} %all-gather.3.cloned.1.call-done, f32[384]{0:T(512)S(1)} %add_rsqrt_fusion.2), kind=kOutput, calls=%fused_computation.30 | convolution fusion | flops 1208254464 | bytes 5899776 | tf_op jit(solution)/shard_map/dot_general | solution.py:117
  147.2 7.0 %convolution_convert_fusion.1 = bf16[384,2048]{1,0:T(8,128)(2,1)} fusion(bf16[768,2048]{0,1:T(8,128)(2,1)S(1)} %bitcast.164, bf16[384,2048]{0,1:T(8,128)(2,1)} %fusion.2, bf16[2048,1536]{1,0:T(8,128)(2,1)} %all-gather.3.cloned.1.call-done, f32[384,768]{1,0:T(8,128)} %fusion.11, f32[384]{0:T(512)S(1)} %add_rsqrt_fusion.2), kind=kOutput, calls=%fused_computation.14 | convolution fusion | flops 2418769920 | bytes 10618368 | tf_op jit(solution)/shard_map/dot_general | solution.py:120
  154.2 2.7 copy.67
  156.9 7.9 %all-to-all-start.2 = ((bf16[8,384,256]{2,1,0:T(8,128)(2,1)}), bf16[8,384,256]{2,1,0:T(8,128)(2,1)S(1)}, u32[]{:S(2)}, u32[]{:S(2)}) async-start(bf16[8,384,256]{2,1,0:T(8,128)(2,1)} %bitcast.147), calls=%async_computation.2 | async-start | bytes 3145728 | tf_op jit(solution)/shard_map/all_to_all | solution.py:50
  165.5 19.8 %all-to-all-done.2 = bf16[8,384,256]{2,1,0:T(8,128)(2,1)S(1)} async-done(((bf16[8,384,256]{2,1,0:T(8,128)(2,1)}), bf16[8,384,256]{2,1,0:T(8,128)(2,1)S(1)}, u32[]{:S(2)}, u32[]{:S(2)}) %all-to-all-start.2) | async-done | bytes 1572896 | tf_op jit(solution)/shard_map/all_to_all | solution.py:50
  186.6 3.6 %all-to-all-start.3 = ((bf16[4,385,256]{2,1,0:T(8,128)(2,1)}), bf16[4,385,256]{2,1,0:T(8,128)(2,1)S(1)}, u32[]{:S(2)}, u32[]{:S(2)}) async-start(bf16[4,385,256]{2,1,0:T(8,128)(2,1)} %broadcast_in_dim.94), calls=%async_computation.3 | async-start | bytes 1605632 | tf_op jit(solution)/shard_map/all_to_all | solution.py:18
  190.3 11.3 %all-to-all-done.3 = bf16[4,385,256]{2,1,0:T(8,128)(2,1)S(1)} async-done(((bf16[4,385,256]{2,1,0:T(8,128)(2,1)}), bf16[4,385,256]{2,1,0:T(8,128)(2,1)S(1)}, u32[]{:S(2)}, u32[]{:S(2)}) %all-to-all-start.3) | async-done | bytes 788512 | tf_op jit(solution)/shard_map/all_to_all | solution.py:18
  202.4 6.5 %all_to_all.51 = bf16[2,4,385,256]{3,1,2,0:T(4,128)(2,1)S(1)} all-to-all(bf16[2,4,385,256]{3,1,2,0:T(4,128)(2,1)S(1)} %broadcast_in_dim.95), channel_id=1, replica_groups=mesh['grp'=2,'fs'=16,'tp_0'=4,'tp_1'=2] {'tp_1'}, dimensions={0} | all-to-all | bytes 3153920 | tf_op jit(solution)/shard_map/all_to_all | solution.py:18
  209.7 4.8 %all-to-all-start.5 = ((bf16[16,128,128]{1,2,0:T(8,128)(2,1)}), bf16[16,128,128]{1,2,0:T(8,128)(2,1)}, u32[]{:S(2)}, u32[]{:S(2)}) async-start(bf16[16,128,128]{1,2,0:T(8,128)(2,1)} %broadcast_in_dim.105), calls=%async_computation.5 | async-start | bytes 1048576 | tf_op jit(solution)/shard_map/all_to_all | solution.py:18
  214.8 1.9 slice_convert_fusion.1
  216.8 3.5 %copy.48 = f32[384,8,256]{0,2,1:T(8,128)} copy(f32[384,8,256]{2,0,1:T(8,128)} %slice_convert_fusion.1) | data formatting | bytes 6291456 | tf_op jit(solution)/shard_map/convert_element_type | solution.py:69
  220.7 2.2 fusion.1
  223.0 3.2 all-gather.5.cloned.1.call-done
  226.1 1.6 fusion.47
  229.4 11.1 %all-to-all-done.5 = bf16[16,128,128]{1,2,0:T(8,128)(2,1)} async-done(((bf16[16,128,128]{1,2,0:T(8,128)(2,1)}), bf16[16,128,128]{1,2,0:T(8,128)(2,1)}, u32[]{:S(2)}, u32[]{:S(2)}) %all-to-all-start.5) | async-done | bytes 524320 | tf_op jit(solution)/shard_map/all_to_all | solution.py:18
  240.5 2.4 convolution_convert_fusion.2
  243.0 30.7 %all_to_all.52 = bf16[8,384,256]{2,1,0:T(8,128)(2,1)S(1)} all-to-all(bf16[8,384,256]{2,1,0:T(8,128)(2,1)S(1)} %bitcast.162), channel_id=1, replica_groups=mesh['grp'=2,'fs'=16,'tp_0'=4,'tp_1'=2] {'tp_0','tp_1'}, dimensions={0} | all-to-all | bytes 3145728 | tf_op jit(solution)/shard_map/all_to_all | solution.py:50
  275.4 13.9 %all_to_all.53 = bf16[4,385,256]{2,1,0:T(8,128)(2,1)S(1)} all-to-all(bf16[4,385,256]{2,1,0:T(8,128)(2,1)S(1)} %broadcast_in_dim.106), channel_id=1, replica_groups=mesh['grp'=2,'fs'=16,'tp_0'=4,'tp_1'=2] {'tp_0'}, dimensions={0} | all-to-all | bytes 1576960 | tf_op jit(solution)/shard_map/all_to_all | solution.py:18
  290.0 6.5 %all_to_all.54 = bf16[2,4,385,256]{3,1,2,0:T(4,128)(2,1)S(1)} all-to-all(bf16[2,4,385,256]{3,1,2,0:T(4,128)(2,1)S(1)} %broadcast_in_dim.107), channel_id=1, replica_groups=mesh['grp'=2,'fs'=16,'tp_0'=4,'tp_1'=2] {'tp_1'}, dimensions={0} | all-to-all | bytes 3153920 | tf_op jit(solution)/shard_map/all_to_all | solution.py:18
  296.8 1.9 slice_convert_fusion
  299.1 2.4 copy.55
  303.0 4.5 %fusion.14 = f32[384,768]{1,0:T(8,128)} fusion(bf16[384,2048]{0,1:T(8,128)(2,1)S(1)} %fusion, bf16[2048,1536]{1,0:T(8,128)(2,1)} %all-gather.3.cloned.1.call-done, f32[384]{0:T(512)S(1)} %add_rsqrt_fusion), kind=kOutput, calls=%fused_computation.31 | convolution fusion | flops 1208254464 | bytes 5899776 | tf_op jit(solution)/shard_map/dot_general | solution.py:117
  307.5 7.0 %convolution_convert_fusion = bf16[384,2048]{1,0:T(8,128)(2,1)} fusion(bf16[768,2048]{0,1:T(8,128)(2,1)S(1)} %bitcast.165, bf16[384,2048]{0,1:T(8,128)(2,1)} %copy-done.3, bf16[2048,1536]{1,0:T(8,128)(2,1)} %all-gather.3.cloned.1.call-done, f32[384,768]{1,0:T(8,128)} %fusion.14, f32[384]{0:T(512)S(1)} %add_rsqrt_fusion), kind=kOutput, calls=%fused_computation.13 | convolution fusion | flops 2418769920 | bytes 10618368 | tf_op jit(solution)/shard_map/dot_general | solution.py:120
  314.5 1.5 copy.65
  316.0 23.6 %all_to_all.55 = bf16[8,384,256]{2,1,0:T(8,128)(2,1)S(1)} all-to-all(bf16[8,384,256]{2,1,0:T(8,128)(2,1)S(1)} %bitcast.163), channel_id=1, replica_groups=mesh['grp'=2,'fs'=16,'tp_0'=4,'tp_1'=2] {'tp_0','tp_1'}, dimensions={0} | all-to-all | bytes 3145728 | tf_op jit(solution)/shard_map/all_to_all | solution.py:50
  (115 shorter events, 27.6 us)
Async XLA Ops:
  6.5 234.0 %copy-start = (bf16[1,128,128]{2,1,0:T(8,128)(2,1)S(1)}, bf16[1,128,128]{2,1,0:T(8,128)(2,1)}, u32[]{:S(2)}) copy-start(bf16[1,128,128]{2,1,0:T(8,128)(2,1)} %param.20) | copy-start | bytes 98308
  6.6 135.6 %all-gather.3.cloned.1.call-start = ((), (), s32[]{:S(2)}) async-start(), calls=%async_computation.10 | async-start | bytes 6684672 | tf_op jit(solution)/shard_map/all_gather | solution.py:60
  8.4 29.4 %collective-permute-start = (bf16[768,128]{1,0:T(8,128)(2,1)}, bf16[768,128]{1,0:T(8,128)(2,1)S(1)}, u32[]{:S(2)}, u32[]{:S(2)}) collective-permute-start(bf16[768,128]{1,0:T(8,128)(2,1)} %param.16), channel_id=1, source_target_pairs={{0,8},{8,16},{16,24},{24,32},{32,40},{40,48},{48,56},{56,64},{64,7... | collective-permute-start | bytes 589832 | tf_op jit(solution)/shard_map/ppermute | solution.py:107
  11.9 26.0 %collective-permute-start.8 = (bf16[768,128]{1,0:T(8,128)(2,1)}, bf16[768,128]{1,0:T(8,128)(2,1)S(1)}, u32[]{:S(2)}, u32[]{:S(2)}) collective-permute-start(bf16[768,128]{1,0:T(8,128)(2,1)} %param.16), channel_id=1, source_target_pairs={{8,0},{16,8},{24,16},{32,24},{40,32},{48,40},{56,48},{64,56},{72,6... | collective-permute-start | bytes 589832 | tf_op jit(solution)/shard_map/ppermute | solution.py:109
  33.5 27.0 %all-to-all-start = ((bf16[4,385,256]{2,1,0:T(8,128)(2,1)}), bf16[4,385,256]{2,1,0:T(8,128)(2,1)S(1)}, u32[]{:S(2)}, u32[]{:S(2)}) async-start(bf16[4,385,256]{2,1,0:T(8,128)(2,1)} %broadcast_in_dim.92), calls=%async_computation | async-start | bytes 1605632 | tf_op jit(solution)/shard_map/all_to_all | solution.py:18
  37.8 8.9 %collective-permute-start.1 = (bf16[768,128]{1,0:T(8,128)(2,1)S(1)}, bf16[768,128]{1,0:T(8,128)(2,1)S(1)}, u32[]{:S(2)}, u32[]{:S(2)}) collective-permute-start(bf16[768,128]{1,0:T(8,128)(2,1)S(1)} %collective-permute-done), channel_id=1, source_target_pairs={{0,8},{8,16},{16,24},{24,32},{32,40},{40,48},{48,56},{56,64},{64,7... | collective-permute-start | bytes 589832 | tf_op jit(solution)/shard_map/ppermute | solution.py:107
  37.9 10.6 %collective-permute-start.9 = (bf16[768,128]{1,0:T(8,128)(2,1)S(1)}, bf16[768,128]{1,0:T(8,128)(2,1)S(1)}, u32[]{:S(2)}, u32[]{:S(2)}) collective-permute-start(bf16[768,128]{1,0:T(8,128)(2,1)S(1)} %collective-permute-done.8), channel_id=1, source_target_pairs={{8,0},{16,8},{24,16},{32,24},{40,32},{48,40},{56,48},{64,56},{72,6... | collective-permute-start | bytes 589832 | tf_op jit(solution)/shard_map/ppermute | solution.py:109
  46.7 11.1 %collective-permute-start.2 = (bf16[768,128]{1,0:T(8,128)(2,1)S(1)}, bf16[768,128]{1,0:T(8,128)(2,1)S(1)}, u32[]{:S(2)}, u32[]{:S(2)}) collective-permute-start(bf16[768,128]{1,0:T(8,128)(2,1)S(1)} %collective-permute-done.1), channel_id=1, source_target_pairs={{0,8},{8,16},{16,24},{24,32},{32,40},{40,48},{48,56},{56,64},{64,7... | collective-permute-start | bytes 589832 | tf_op jit(solution)/shard_map/ppermute | solution.py:107
  48.5 10.5 %collective-permute-start.10 = (bf16[768,128]{1,0:T(8,128)(2,1)S(1)}, bf16[768,128]{1,0:T(8,128)(2,1)S(1)}, u32[]{:S(2)}, u32[]{:S(2)}) collective-permute-start(bf16[768,128]{1,0:T(8,128)(2,1)S(1)} %collective-permute-done.9), channel_id=1, source_target_pairs={{8,0},{16,8},{24,16},{32,24},{40,32},{48,40},{56,48},{64,56},{72,6... | collective-permute-start | bytes 589832 | tf_op jit(solution)/shard_map/ppermute | solution.py:109
  57.8 19.2 %collective-permute-start.3 = (bf16[768,128]{1,0:T(8,128)(2,1)S(1)}, bf16[768,128]{1,0:T(8,128)(2,1)S(1)}, u32[]{:S(2)}, u32[]{:S(2)}) collective-permute-start(bf16[768,128]{1,0:T(8,128)(2,1)S(1)} %collective-permute-done.2), channel_id=1, source_target_pairs={{0,8},{8,16},{16,24},{24,32},{32,40},{40,48},{48,56},{56,64},{64,7... | collective-permute-start | bytes 589832 | tf_op jit(solution)/shard_map/ppermute | solution.py:107
  59.0 33.8 %collective-permute-start.11 = (bf16[768,128]{1,0:T(8,128)(2,1)S(1)}, bf16[768,128]{1,0:T(8,128)(2,1)S(1)}, u32[]{:S(2)}, u32[]{:S(2)}) collective-permute-start(bf16[768,128]{1,0:T(8,128)(2,1)S(1)} %collective-permute-done.10), channel_id=1, source_target_pairs={{8,0},{16,8},{24,16},{32,24},{40,32},{48,40},{56,48},{64,56},{72,6... | collective-permute-start | bytes 589832 | tf_op jit(solution)/shard_map/ppermute | solution.py:109
  77.0 12.3 %collective-permute-start.4 = (bf16[768,128]{1,0:T(8,128)(2,1)S(1)}, bf16[768,128]{1,0:T(8,128)(2,1)S(1)}, u32[]{:S(2)}, u32[]{:S(2)}) collective-permute-start(bf16[768,128]{1,0:T(8,128)(2,1)S(1)} %collective-permute-done.3), channel_id=1, source_target_pairs={{0,8},{8,16},{16,24},{24,32},{32,40},{40,48},{48,56},{56,64},{64,7... | collective-permute-start | bytes 589832 | tf_op jit(solution)/shard_map/ppermute | solution.py:107
  89.4 12.1 %collective-permute-start.5 = (bf16[768,128]{1,0:T(8,128)(2,1)S(1)}, bf16[768,128]{1,0:T(8,128)(2,1)S(1)}, u32[]{:S(2)}, u32[]{:S(2)}) collective-permute-start(bf16[768,128]{1,0:T(8,128)(2,1)S(1)} %collective-permute-done.4), channel_id=1, source_target_pairs={{0,8},{8,16},{16,24},{24,32},{32,40},{40,48},{48,56},{56,64},{64,7... | collective-permute-start | bytes 589832 | tf_op jit(solution)/shard_map/ppermute | solution.py:107
  92.7 37.9 %copy-start.8 = (bf16[768,128]{1,0:T(8,128)(2,1)S(1)}, bf16[768,128]{1,0:T(8,128)(2,1)}, u32[]{:S(2)}) copy-start(bf16[768,128]{1,0:T(8,128)(2,1)} %param.16) | copy-start | bytes 589828
  92.7 9.2 %collective-permute-start.12 = (bf16[768,128]{1,0:T(8,128)(2,1)S(1)}, bf16[768,128]{1,0:T(8,128)(2,1)S(1)}, u32[]{:S(2)}, u32[]{:S(2)}) collective-permute-start(bf16[768,128]{1,0:T(8,128)(2,1)S(1)} %collective-permute-done.11), channel_id=1, source_target_pairs={{8,0},{16,8},{24,16},{32,24},{40,32},{48,40},{56,48},{64,56},{72,6... | collective-permute-start | bytes 589832 | tf_op jit(solution)/shard_map/ppermute | solution.py:109
  101.5 11.9 %collective-permute-start.6 = (bf16[768,128]{1,0:T(8,128)(2,1)S(1)}, bf16[768,128]{1,0:T(8,128)(2,1)S(1)}, u32[]{:S(2)}, u32[]{:S(2)}) collective-permute-start(bf16[768,128]{1,0:T(8,128)(2,1)S(1)} %collective-permute-done.5), channel_id=1, source_target_pairs={{0,8},{8,16},{16,24},{24,32},{32,40},{40,48},{48,56},{56,64},{64,7... | collective-permute-start | bytes 589832 | tf_op jit(solution)/shard_map/ppermute | solution.py:107
  101.9 11.5 %collective-permute-start.13 = (bf16[768,128]{1,0:T(8,128)(2,1)S(1)}, bf16[768,128]{1,0:T(8,128)(2,1)S(1)}, u32[]{:S(2)}, u32[]{:S(2)}) collective-permute-start(bf16[768,128]{1,0:T(8,128)(2,1)S(1)} %collective-permute-done.12), channel_id=1, source_target_pairs={{8,0},{16,8},{24,16},{32,24},{40,32},{48,40},{56,48},{64,56},{72,6... | collective-permute-start | bytes 589832 | tf_op jit(solution)/shard_map/ppermute | solution.py:109
  113.4 11.7 %collective-permute-start.7 = (bf16[768,128]{1,0:T(8,128)(2,1)S(1)}, bf16[768,128]{1,0:T(8,128)(2,1)S(1)}, u32[]{:S(2)}, u32[]{:S(2)}) collective-permute-start(bf16[768,128]{1,0:T(8,128)(2,1)S(1)} %collective-permute-done.6), channel_id=1, source_target_pairs={{0,8},{8,16},{16,24},{24,32},{32,40},{40,48},{48,56},{56,64},{64,7... | collective-permute-start | bytes 589832 | tf_op jit(solution)/shard_map/ppermute | solution.py:107
  113.4 22.1 %collective-permute-start.14 = (bf16[768,128]{1,0:T(8,128)(2,1)S(1)}, bf16[768,128]{1,0:T(8,128)(2,1)S(1)}, u32[]{:S(2)}, u32[]{:S(2)}) collective-permute-start(bf16[768,128]{1,0:T(8,128)(2,1)S(1)} %collective-permute-done.13), channel_id=1, source_target_pairs={{8,0},{16,8},{24,16},{32,24},{40,32},{48,40},{56,48},{64,56},{72,6... | collective-permute-start | bytes 589832 | tf_op jit(solution)/shard_map/ppermute | solution.py:109
  142.2 5.0 %copy-start.1 = (bf16[768,16,128]{0,2,1:T(8,128)(2,1)S(1)}, bf16[768,16,128]{0,2,1:T(8,128)(2,1)}, u32[]{:S(2)}) copy-start(bf16[768,16,128]{0,2,1:T(8,128)(2,1)} %copy.44) | copy-start | bytes 9437188
  154.2 10.6 %copy-start.9 = (bf16[128,256]{1,0:T(8,128)(2,1)S(1)}, bf16[128,256]{1,0:T(8,128)(2,1)}, u32[]{:S(2)}) copy-start(bf16[128,256]{1,0:T(8,128)(2,1)} %param.19) | copy-start | bytes 196612
  154.2 10.6 %copy-start.11 = (bf16[128,128]{1,0:T(8,128)(2,1)S(1)}, bf16[128,128]{1,0:T(8,128)(2,1)}, u32[]{:S(2)}) copy-start(bf16[128,128]{1,0:T(8,128)(2,1)} %param.18) | copy-start | bytes 98308
  156.9 28.7 %copy-start.4 = (bf16[384,256]{1,0:T(8,128)(2,1)S(1)}, bf16[384,256]{1,0:T(8,128)(2,1)}, u32[]{:S(2)}) copy-start(bf16[384,256]{1,0:T(8,128)(2,1)} %param.12) | copy-start | bytes 589828
  156.9 28.7 %copy-start.12 = (bf16[1,256]{1,0:T(2,128)(2,1)S(1)}, bf16[1,256]{1,0:T(2,128)(2,1)}, u32[]{:S(2)}) copy-start(bf16[1,256]{1,0:T(2,128)(2,1)} %param.17) | copy-start | bytes 1540
  156.9 28.4 %all-to-all-start.2 = ((bf16[8,384,256]{2,1,0:T(8,128)(2,1)}), bf16[8,384,256]{2,1,0:T(8,128)(2,1)S(1)}, u32[]{:S(2)}, u32[]{:S(2)}) async-start(bf16[8,384,256]{2,1,0:T(8,128)(2,1)} %bitcast.147), calls=%async_computation.2 | async-start | bytes 3145728 | tf_op jit(solution)/shard_map/all_to_all | solution.py:50
  164.7 25.5 %copy-start.10 = (bf16[128,128]{1,0:T(8,128)(2,1)S(1)}, bf16[128,128]{1,0:T(8,128)(2,1)}, u32[]{:S(2)}) copy-start(bf16[128,128]{1,0:T(8,128)(2,1)} %param.22) | copy-start | bytes 98308
  164.7 61.4 %all-gather.5.cloned.1.call-start = ((), (), s32[]{:S(2)}) async-start(), calls=%async_computation.11 | async-start | bytes 1671168 | tf_op jit(solution)/shard_map/all_gather | solution.py:60
  186.6 15.1 %all-to-all-start.3 = ((bf16[4,385,256]{2,1,0:T(8,128)(2,1)}), bf16[4,385,256]{2,1,0:T(8,128)(2,1)S(1)}, u32[]{:S(2)}, u32[]{:S(2)}) async-start(bf16[4,385,256]{2,1,0:T(8,128)(2,1)} %broadcast_in_dim.94), calls=%async_computation.3 | async-start | bytes 1605632 | tf_op jit(solution)/shard_map/all_to_all | solution.py:18
  209.7 30.8 %all-to-all-start.5 = ((bf16[16,128,128]{1,2,0:T(8,128)(2,1)}), bf16[16,128,128]{1,2,0:T(8,128)(2,1)}, u32[]{:S(2)}, u32[]{:S(2)}) async-start(bf16[16,128,128]{1,2,0:T(8,128)(2,1)} %broadcast_in_dim.105), calls=%async_computation.5 | async-start | bytes 1048576 | tf_op jit(solution)/shard_map/all_to_all | solution.py:18
  222.9 17.6 %copy-start.15 = (f32[1,128]{1,0:T(1,128)S(1)}, f32[1,128]{1,0:T(1,128)}, u32[]{:S(2)}) copy-start(f32[1,128]{1,0:T(1,128)} %param.21) | copy-start | bytes 1540
  227.8 0.7 copy-start.7
  243.0 30.9 %copy-start.14 = (bf16[2048,384]{1,0:T(8,128)(2,1)S(1)}, bf16[2048,384]{1,0:T(8,128)(2,1)}, u32[]{:S(2)}) copy-start(bf16[2048,384]{1,0:T(8,128)(2,1)} %all-gather.5.cloned.1.call-done) | copy-start | bytes 4718596
  273.9 0.7 copy-start.13
  274.6 0.7 copy-start.5
  301.8 1.1 copy-start.3
  303.0 4.5 %copy-start.2 = (bf16[768,16,128]{0,2,1:T(8,128)(2,1)S(1)}, bf16[768,16,128]{0,2,1:T(8,128)(2,1)}, u32[]{:S(2)}) copy-start(bf16[768,16,128]{0,2,1:T(8,128)(2,1)} %copy.44) | copy-start | bytes 9437188
  316.0 23.8 %copy-start.6 = (bf16[384,256]{1,0:T(8,128)(2,1)S(1)}, bf16[384,256]{1,0:T(8,128)(2,1)}, u32[]{:S(2)}) copy-start(bf16[384,256]{1,0:T(8,128)(2,1)} %copy-done.5) | copy-start | bytes 589828
Sparse Core Ops, SparseCore 0:
  9.1 125.9 all-gather.2
  167.3 58.7 all-gather.4
